TPU v7x, 512 devices: a whole 4x4x16 slice. The times are simulated.
512 devices in a mesh: sp: 64 (over z, y), dp: 8 (over x, core).
Axes of the slice: x: 4, y: 4, z: 16, core: 2. Of those that a mesh axis runs over, the one named last changes fastest.
Arguments:
- val_input: bfloat16 [8192, 1536], P('sp', 'dp'), may hold values from -24 to 24, as said below
- gate_input: bfloat16 [8192, 1536], P('sp', 'dp'), may hold values from -8 to 8
- cotangent: bfloat16 [8192, 4096], P('sp'), may hold values from -16 to 16
- out_weight: bfloat16 [4096, 1536], P('sp', 'dp'), may hold values from -0.09375 to 0.09375
- conv_taps: float32 [31, 1536], P(None, 'dp'), may hold values from -1 to 1
- norm_gain: float32 [1536], P('dp'), may hold values from 0.1 to 1.9
Outputs:
- grad_val: bfloat16 [8192, 1536], P('sp', 'dp')
- grad_gate: bfloat16 [8192, 1536], P('sp', 'dp')
- grad_out_weight: float32 [4096, 1536], P('sp', 'dp')
- grad_taps: float32 [31, 1536], P(None, 'dp')
- grad_gain: float32 [1536], P('dp')
Inputs may be any that keep to these rules, and one draw needn't show every extreme that they name: `val_input`: blocks of 64 channels and blocks of 32 tokens carry their own scales.
All inputs are finite; a program needn't handle non-finite values.
Results may differ from a plain program's by a relative error of at most 0.0063.
Values may be sent and summed in bfloat16 or wider, within the bound.
No kernel may reach another device: no remote copies, remote signals or barrier semaphores. Data moves between devices by JAX's collectives and lax.ppermute only.
A program may use at most 64 MiB of HBM per device.

v0:
```python
import jax
import jax.numpy as jnp
from jax import lax
from jax.sharding import Mesh
from jax.sharding import PartitionSpec as P

SP = ("sp_0", "sp_1")
norm_floor = 0.25


def whole_of(array, axes, dim):
    if not axes:
        return array
    nearer = lax.all_gather(array, axes[-1], axis=dim, tiled=True)
    return whole_of(nearer, axes[:-1], dim)


def passed_along(value, axis, steps):
    count = lax.axis_size(axis)
    first, last = (max(0, -steps), min(count, count - steps))
    return lax.ppermute(value, axis, [(source, source + steps) for source in range(first, last)])


def from_everyone(array, axis):
    copies = jnp.broadcast_to(array, (lax.axis_size(axis), *array.shape))
    return lax.all_to_all(copies, axis, split_axis=0, concat_axis=0, tiled=True)


def taken_together(array, axis):
    return from_everyone(array, axis).sum(axis=0)


def packed_total(arrays, axis):
    ravelled, at, finished = (jnp.concatenate([a.reshape(-1) for a in arrays]), 0, [])
    running = taken_together(ravelled, axis)
    for a in arrays:
        finished.append(running[at : at + a.size].reshape(a.shape))
        at += a.size
    return tuple(finished)


def own_block(blocks, axes, turns):
    lengths = [lax.axis_size(a) for a in axes]
    blocks = blocks.reshape(*lengths, *blocks.shape[1:])
    blocks = blocks.transpose(*turns, *range(len(axes), blocks.ndim))
    blocks = blocks.reshape(-1, *blocks.shape[len(axes) :])
    for k in turns:
        blocks = lax.psum_scatter(blocks, axes[k], scatter_dimension=0, tiled=True)
    return blocks[0]


def split_up(array, dim, length):
    lengths = array.shape
    blocks = array.reshape(*lengths[:dim], length, lengths[dim] // length, *lengths[dim + 1 :])
    return jnp.moveaxis(blocks, dim, 0)


def scatter_axes(array, axes, turns, dim):
    length = lax.axis_size(axes)
    return own_block(split_up(array, dim, length), axes, turns)


def by_axis(array, axes):
    for axis in axes:
        array = lax.psum(array, axis)
    return array


def per_device(val_input, gate_input, cotangent, out_weight, conv_taps, norm_gain):
    rows_here = val_input.shape[0]
    width_dp = val_input.shape[1]
    taps = conv_taps.shape[0]
    channels = width_dp * lax.axis_size("dp")
    columns = cotangent
    grad_mix = jnp.dot(columns, whole_of(out_weight, SP, 0), preferred_element_type=jnp.float32)
    sigma_gate = jax.nn.sigmoid(gate_input.astype(jnp.float32))
    mixed_in = (val_input.astype(jnp.float32) * sigma_gate).astype(jnp.bfloat16)
    earlier = passed_along(mixed_in[rows_here - (taps - 1) :], SP, 1)
    padded_in = jnp.concatenate([earlier, lax.optimization_barrier(mixed_in)], 0).astype(
        jnp.float32
    )
    conv_out = jnp.zeros((rows_here, width_dp), jnp.float32)
    for offset in range(taps):
        conv_out = conv_out + conv_taps[offset][None, :] * padded_in[offset : offset + rows_here]
    conv_rows = lax.optimization_barrier(conv_out.astype(jnp.bfloat16)).astype(jnp.float32)
    row_sums = packed_total((jnp.sum(conv_rows, 1), jnp.sum(conv_rows * conv_rows, 1)), "dp")
    row_mean = row_sums[0][:, None] / channels
    row_var = row_sums[1][:, None] / channels - row_mean * row_mean
    inv_scale = lax.rsqrt(row_var + norm_floor)
    normed = (conv_rows - row_mean) * inv_scale
    act = normed * norm_gain[None, :]
    sigma_act = jax.nn.sigmoid(act)
    swished = (act * sigma_act).astype(jnp.bfloat16)
    columns = cotangent
    grad_out_weight = scatter_axes(
        lax.dot_general(
            columns, swished, (((0,), (0,)), ((), ())), preferred_element_type=jnp.float32
        ),
        SP,
        (1, 0),
        0,
    )
    grad_act = grad_mix * sigma_act * (1.0 + act * (1.0 - sigma_act))
    gain_part = jnp.sum(grad_act * normed, 0)
    grad_norm = grad_act * norm_gain[None, :]
    norm_sums = packed_total((jnp.sum(grad_norm, 1), jnp.sum(grad_norm * normed, 1)), "dp")
    first_sum = norm_sums[0][:, None] / channels
    second_sum = norm_sums[1][:, None] / channels
    grad_conv = (inv_scale * (grad_norm - first_sum - normed * second_sum)).astype(jnp.bfloat16)
    later = passed_along(grad_conv[: taps - 1], SP, -1)
    padded_grad = jnp.concatenate([lax.optimization_barrier(grad_conv), later], 0).astype(
        jnp.float32
    )
    own_grad = padded_grad[:rows_here]
    grad_mixed = jnp.zeros((rows_here, width_dp), jnp.float32)
    tap_list = []
    for offset in range(taps):
        back = taps - 1 - offset
        grad_mixed = grad_mixed + conv_taps[offset][None, :] * padded_grad[back : back + rows_here]
        tap_list.append(jnp.sum(own_grad * padded_in[offset : offset + rows_here], 0))
    grad_taps, grad_gain = (by_axis(jnp.stack(tap_list, 0), SP), by_axis(gain_part, SP))
    grad_rows = lax.optimization_barrier(grad_mixed.astype(jnp.bfloat16)).astype(jnp.float32)
    grad_val = (grad_rows * sigma_gate).astype(jnp.bfloat16)
    grad_gate = (
        grad_rows * val_input.astype(jnp.float32) * sigma_gate * (1.0 - sigma_gate)
    ).astype(jnp.bfloat16)
    return (grad_val, grad_gate, grad_out_weight, grad_taps, grad_gain)


def solution(mesh):
    split = Mesh(mesh.devices.reshape(16, 4, mesh.shape["dp"]), ("sp_0", "sp_1", "dp"))
    in_specs = (P(SP, "dp"), P(SP, "dp"), P(SP, None), P(SP, "dp"), P(None, "dp"), P("dp"))
    out_specs = (P(SP, "dp"), P(SP, "dp"), P(SP, "dp"), P(None, "dp"), P("dp"))
    return jax.shard_map(
        per_device, mesh=split, in_specs=in_specs, out_specs=out_specs, check_vma=False
    )
```

profile of v0, /device:TPU:2, one launch (start us, length us, event | category | flops | bytes accessed | tf_op | source)
XLA Modules:
  0.0 214.0 jit_solution(13165765928091978181)
XLA Ops:
  8.0 0.0 copy-start
  8.0 0.0 copy-start.3
  8.0 0.0 all-gather.2.cloned.1.call-start
  8.1 14.2 %all_gather.6 = bf16[256,192]{1,0:T(8,128)(2,1)} all-gather(bf16[64,192]{1,0:T(8,128)(2,1)} %param.9), channel_id=1, replica_groups=mesh['sp_0'=16,'sp_1'=4,'dp'=8] {'sp_1'}, dimensions={0}, use_global_device_ids=true | all-gather | bytes 122880 | tf_op jit(solution)/shard_map/all_gather | solution.py:14
  22.3 0.0 all-gather.2.cloned.1.call-update
  22.3 0.0 reduce-scatter.3.cloned.1.call-start
  22.4 0.9 fusion.1
  23.2 0.1 slice.459
  23.3 2.6 %collective-permute-start = (bf16[30,192]{0,1:T(8,128)(2,1)S(1)}, bf16[30,192]{0,1:T(8,128)(2,1)S(1)}, u32[]{:S(2)}, u32[]{:S(2)}) collective-permute-start(bf16[30,192]{0,1:T(8,128)(2,1)S(1)} %slice.459), channel_id=1, source_target_pairs={{0,8},{8,16},{16,24},{24,32},{32,40},{40,48},{48,56},{56,64},{64,7... | collective-permute-start | bytes 34568 | tf_op jit(solution)/shard_map/ppermute | solution.py:21
  25.9 1.1 fusion.62
  27.0 1.0 fusion.63
  27.9 0.0 collective-permute-done
  28.0 0.1 maximum_convert_fusion
  28.1 1.8 add_convert_fusion
  29.9 10.4 %all_to_all.12 = f32[8,1,256]{2,1,0:T(1,128)S(1)} all-to-all(f32[8,1,256]{2,1,0:T(1,128)S(1)} %broadcast_in_dim.4), channel_id=1, replica_groups=mesh['sp_0'=16,'sp_1'=4,'dp'=8] {'dp'}, dimensions={0} | all-to-all | bytes 16384 | tf_op jit(solution)/shard_map/all_to_all | solution.py:26
  40.4 0.0 copy-done
  40.4 0.0 copy-done.3
  40.4 2.3 %convolution_bitcast_fusion = f32[4096,192]{0,1:T(8,128)} fusion(bf16[128,4096]{1,0:T(8,128)(2,1)S(1)} %copy-done, bf16[128,192]{0,1:T(8,128)(2,1)S(1)} %add_convert_fusion, f32[192]{0:T(256)S(1)} %copy-done.3, f32[128]{0:T(128)S(1)} %get-tuple-element.85, f32[128]{0:T(128)S(1)} %get-tuple-element.84), kind=kOutput, calls=%fused_computation | convolution fusion | flops 201547776 | bytes 4245248 | tf_op jit(solution)/shard_map/dot_general | solution.py:96
  42.7 5.1 %copy.19 = f32[4096,192]{1,0:T(8,128)} copy(f32[4096,192]{0,1:T(8,128)} %convolution_bitcast_fusion) | data formatting | bytes 6291456 | tf_op jit(solution)/shard_map/dot_general | solution.py:96
  47.9 4.6 %copy.20 = f32[4,16,64,192]{3,2,1,0:T(8,128)} copy(f32[4,16,64,192]{3,2,0,1:T(8,128)} %bitcast.73) | data formatting | bytes 6291456 | tf_op jit(solution)/shard_map/transpose | solution.py:45
  52.5 0.0 reduce-scatter.3.cloned.1.call-update
  52.5 0.0 reduce-scatter.5.cloned.1.call-start
  52.6 45.5 %all-gather.2.cloned.1.call-done = bf16[4096,192]{1,0:T(8,128)(2,1)} async-done(((bf16[256,192]{1,0:T(8,128)(2,1)}), bf16[4096,192]{1,0:T(8,128)(2,1)}) %all-gather.2.cloned.1.call-update) | async-done | bytes 1572880 | tf_op jit(solution)/shard_map/all_gather | solution.py:14
  98.1 2.5 %fusion.24 = (f32[192]{0:T(256)S(1)}, f32[128]{0:T(128)S(1)}, f32[128]{0:T(128)S(1)}, f32[128,192]{0,1:T(8,128)S(1)}) fusion(bf16[128,192]{0,1:T(8,128)(2,1)S(1)} %add_convert_fusion, f32[128]{0:T(128)S(1)} %get-tuple-element.85, f32[128]{0:T(128)S(1)} %get-tuple-element.84, f32[192]{0:T(256)S(1)} %copy-done.3, bf16[128,4096]{1,0:T(8,128)(2,1)S(1)} %copy-done, ...), kind=kOutput, calls=%fused_computation.32 | convolution fusion | flops 201768512 | bytes 2772480 | tf_op jit(solution)/shard_map/dot_general | solution.py:75
  100.6 10.0 %reduce-scatter.3.cloned.1.call-done = f32[16,64,192]{2,1,0:T(8,128)} async-done(((f32[64,64,192]{2,1,0:T(8,128)}), f32[16,64,192]{2,1,0:T(8,128)}) %reduce-scatter.3.cloned.1.call-update) | async-done | bytes 786448 | tf_op jit(solution)/shard_map/reduce_scatter | solution.py:48
  110.7 0.0 reduce-scatter.5.cloned.1.call-update
  110.7 8.5 %all_to_all.13 = f32[8,1,256]{2,1,0:T(1,128)S(1)} all-to-all(f32[8,1,256]{2,1,0:T(1,128)S(1)} %broadcast_in_dim.5), channel_id=1, replica_groups=mesh['sp_0'=16,'sp_1'=4,'dp'=8] {'dp'}, dimensions={0} | all-to-all | bytes 16384 | tf_op jit(solution)/shard_map/all_to_all | solution.py:26
  119.2 0.1 fusion.23
  119.3 1.3 collective-permute-start.1
  120.6 4.7 %collective-permute-done.1 = bf16[30,192]{0,1:T(8,128)(2,1)S(1)} collective-permute-done((bf16[30,192]{0,1:T(8,128)(2,1)S(1)}, bf16[30,192]{0,1:T(8,128)(2,1)S(1)}, u32[]{:S(2)}, u32[]{:S(2)}) %collective-permute-start.1) | collective-permute-done | bytes 11552 | tf_op jit(solution)/shard_map/ppermute | solution.py:21
  125.3 0.0 copy-start.1
  125.4 0.0 copy-start.2
  125.4 1.8 fusion.27
  127.2 0.7 multiply_reduce_fusion.18
  127.9 0.7 multiply_reduce_fusion.9
  128.5 0.9 multiply_reduce_fusion
  129.4 0.1 stack.127
  129.5 57.1 %all-reduce = (f32[31,192]{1,0:T(8,128)S(1)}, f32[192]{0:T(256)S(1)}) all-reduce(f32[31,192]{1,0:T(8,128)S(1)} %stack.127, f32[192]{0:T(256)S(1)} %get-tuple-element.36), channel_id=1, replica_groups=mesh['sp_0'=16,'sp_1'=4,'dp'=8] {'sp_0'}, use_global_device_ids=true, to_apply=%region_39.0 | all-reduce | flops 6144 | bytes 49152 | tf_op jit(solution)/shard_map/psum | solution.py:65
  186.6 19.2 %all-reduce.1 = (f32[31,192]{1,0:T(8,128)}, f32[192]{0:T(256)}) all-reduce(f32[31,192]{1,0:T(8,128)S(1)} %get-tuple-element.41, f32[192]{0:T(256)S(1)} %get-tuple-element.42), channel_id=1, replica_groups=mesh['sp_0'=16,'sp_1'=4,'dp'=8] {'sp_1'}, use_global_device_ids=true, to_apply=%region_40.0 | all-reduce | flops 6144 | bytes 49152 | tf_op jit(solution)/shard_map/psum | solution.py:65
  205.8 0.0 copy-done.1
  205.8 0.0 copy-done.2
  205.8 0.7 fusion.5
  206.5 0.0 reduce-scatter.5.cloned.1.call-done
  (10 shorter events, 0.2 us)
Async XLA Ops:
  8.0 32.4 %copy-start = (bf16[128,4096]{1,0:T(8,128)(2,1)S(1)}, bf16[128,4096]{1,0:T(8,128)(2,1)}, u32[]{:S(2)}) copy-start(bf16[128,4096]{1,0:T(8,128)(2,1)} %param.8) | copy-start | bytes 3145732
  8.0 32.4 %copy-start.3 = (f32[192]{0:T(256)S(1)}, f32[192]{0:T(256)}, u32[]{:S(2)}) copy-start(f32[192]{0:T(256)} %param.11) | copy-start | bytes 2308
  8.0 90.1 %all-gather.2.cloned.1.call-start = ((), (), s32[]{:S(2)}) async-start(), calls=%async_computation.4 | async-start | bytes 2228224 | tf_op jit(solution)/shard_map/all_gather | solution.py:14
  22.3 88.4 %reduce-scatter.3.cloned.1.call-start = ((), (), s32[]{:S(2)}) async-start(), calls=%async_computation.5 | async-start | bytes 5242880 | tf_op jit(solution)/shard_map/reduce_scatter | solution.py:48
  23.3 4.6 %collective-permute-start = (bf16[30,192]{0,1:T(8,128)(2,1)S(1)}, bf16[30,192]{0,1:T(8,128)(2,1)S(1)}, u32[]{:S(2)}, u32[]{:S(2)}) collective-permute-start(bf16[30,192]{0,1:T(8,128)(2,1)S(1)} %slice.459), channel_id=1, source_target_pairs={{0,8},{8,16},{16,24},{24,32},{32,40},{40,48},{48,56},{56,64},{64,7... | collective-permute-start | bytes 34568 | tf_op jit(solution)/shard_map/ppermute | solution.py:21
  52.5 154.0 %reduce-scatter.5.cloned.1.call-start = ((), (), s32[]{:S(2)}) async-start(), calls=%async_computation.6 | async-start | bytes 1114112 | tf_op jit(solution)/shard_map/reduce_scatter | solution.py:48
  119.3 6.0 %collective-permute-start.1 = (bf16[30,192]{0,1:T(8,128)(2,1)S(1)}, bf16[30,192]{0,1:T(8,128)(2,1)S(1)}, u32[]{:S(2)}, u32[]{:S(2)}) collective-permute-start(bf16[30,192]{0,1:T(8,128)(2,1)S(1)} %bitcast.75), channel_id=1, source_target_pairs={{8,0},{16,8},{24,16},{32,24},{40,32},{48,40},{56,48},{64,56},{72,6... | collective-permute-start | bytes 34568 | tf_op jit(solution)/shard_map/ppermute | solution.py:21
  125.3 80.5 %copy-start.1 = (bf16[128,192]{0,1:T(8,128)(2,1)S(1)}, bf16[128,192]{0,1:T(8,128)(2,1)}, u32[]{:S(2)}) copy-start(bf16[128,192]{0,1:T(8,128)(2,1)} %param.6) | copy-start | bytes 147460
  125.4 80.5 %copy-start.2 = (bf16[128,192]{0,1:T(8,128)(2,1)S(1)}, bf16[128,192]{0,1:T(8,128)(2,1)}, u32[]{:S(2)}) copy-start(bf16[128,192]{0,1:T(8,128)(2,1)} %param.7) | copy-start | bytes 147460
Sparse Core Ops, SparseCore 0:
  22.4 75.6 all-gather.1
  110.8 71.1 reduce-scatter.4
Sparse Core Ops, SparseCore 1:
  52.6 58.0 reduce-scatter.2
where the time goes:
time: 215 us; the launch traced here: 214 us
  blocking collectives  109 us (51%)
  waiting for transfers between devices  60.3 us (28%)
  between operations  15.6 us (7%)
  local copies, waits for them, and re-layouts  12 us (6%)
  other arithmetic  7.74 us (4%)
  matrix products  4.84 us (2%)
  starting transfers between devices  3.98 us (2%)
    psum x2, blocking collectives, by_axis(): array = lax.psum(array, axis)  76.3 us
    all_gather x1, waiting for transfers between devices, whole_of(): nearer = lax.all_gather(array, axes[-1], axis=dim, tiled=True)  45.5 us
    all_to_all x2, blocking collectives, from_everyone(): return lax.all_to_all(copies, axis, split_axis=0, concat_axis=0, tiled=True)  18.9 us
    all_gather x1, blocking collectives, whole_of(): nearer = lax.all_gather(array, axes[-1], axis=dim, tiled=True)  14.2 us
    reduce_scatter x2, waiting for transfers between devices, own_block(): blocks = lax.psum_scatter(blocks, axes[k], scatter_dimension=0, tiled=True)  10 us
    dot_general x1, local copies, waits for them, and re-layouts, per_device(): lax.dot_general(columns, swished, (((0,), (0,)), ((), ())), preferred_ele...  5.12 us
    ppermute x2, waiting for transfers between devices, passed_along(): lax.ppermute(value, axis, [(source, source + steps) for source in range(f...  4.69 us
    transpose x1, local copies, waits for them, and re-layouts, own_block(): blocks = blocks.transpose(*turns, *range(len(axes), blocks.ndim))  4.64 us
  transfers between devices with their start and end apart: 5, of which 3 were waited for; matrix products, arithmetic and copies ran while one was open for 11% of the time, Pallas kernels for 0%

commit v1 on v0

--- a/solution.py
+++ b/solution.py
@@ -62,7 +62,7 @@
 
 def by_axis(array, axes):
     for axis in axes:
-        array = lax.psum(array, axis)
+        array = jnp.sum(lax.all_gather(array, axis), axis=0)
     return array
 
 

time: 215 us -> 236 us (1.098)
  the two profiles are of different devices: /device:TPU:2 before, /device:TPU:6 now
where the time goes in v1:
time: 236 us; the launch traced here: 235 us
  blocking collectives  133 us (56%)
  waiting for transfers between devices  46.5 us (20%)
  between operations  16.9 us (7%)
  local copies, waits for them, and re-layouts  15.8 us (7%)
  other arithmetic  9.02 us (4%)
  starting transfers between devices  8.99 us (4%)
  matrix products  4.84 us (2%)
    unnamed x2, blocking collectives  67.2 us
    all_gather x1, waiting for transfers between devices, whole_of(): nearer = lax.all_gather(array, axes[-1], axis=dim, tiled=True)  46.2 us
    all_gather x2, blocking collectives, by_axis(): array = jnp.sum(lax.all_gather(array, axis), axis=0)  41.6 us
    all_gather x1, blocking collectives, whole_of(): nearer = lax.all_gather(array, axes[-1], axis=dim, tiled=True)  14.2 us
    all_to_all x1, blocking collectives, from_everyone(): return lax.all_to_all(copies, axis, split_axis=0, concat_axis=0, tiled=True)  9.77 us
    dot_general x1, local copies, waits for them, and re-layouts, per_device(): lax.dot_general(columns, swished, (((0,), (0,)), ((), ())), preferred_ele...  5.12 us
    all_to_all x1, starting transfers between devices, from_everyone(): return lax.all_to_all(copies, axis, split_axis=0, concat_axis=0, tiled=True)  5.06 us
  transfers between devices with their start and end apart: 6, of which 2 were waited for; matrix products, arithmetic and copies ran while one was open for 13% of the time, Pallas kernels for 0%

profile of v1, /device:TPU:6, one launch (start us, length us, event | category | flops | bytes accessed | tf_op | source)
XLA Modules:
  0.0 235.0 jit_solution(5134357420061384319)
XLA Ops:
  8.0 0.0 copy-start
  8.0 0.0 copy-start.3
  8.0 0.0 all-gather.8.cloned.1.call-start
  8.1 14.2 %all_gather.30 = bf16[256,192]{1,0:T(8,128)(2,1)} all-gather(bf16[64,192]{1,0:T(8,128)(2,1)} %param.9), channel_id=1, replica_groups=mesh['sp_0'=16,'sp_1'=4,'dp'=8] {'sp_1'}, dimensions={0}, use_global_device_ids=true | all-gather | bytes 122880 | tf_op jit(solution)/shard_map/all_gather | solution.py:14
  22.3 0.0 all-gather.8.cloned.1.call-update
  22.3 0.0 reduce-scatter.3.cloned.1.call-start
  22.4 0.9 fusion.1
  23.2 0.1 slice.459
  23.3 2.6 %collective-permute-start = (bf16[30,192]{0,1:T(8,128)(2,1)S(1)}, bf16[30,192]{0,1:T(8,128)(2,1)S(1)}, u32[]{:S(2)}, u32[]{:S(2)}) collective-permute-start(bf16[30,192]{0,1:T(8,128)(2,1)S(1)} %slice.459), channel_id=1, source_target_pairs={{0,8},{8,16},{16,24},{24,32},{32,40},{40,48},{48,56},{56,64},{64,7... | collective-permute-start | bytes 34568 | tf_op jit(solution)/shard_map/ppermute | solution.py:21
  25.9 1.0 fusion.62
  26.9 1.0 fusion.63
  27.9 0.0 collective-permute-done
  27.9 0.1 maximum_convert_fusion
  28.0 1.8 add_convert_fusion
  29.9 9.8 %all_to_all.12 = f32[8,1,256]{2,1,0:T(1,128)S(1)} all-to-all(f32[8,1,256]{2,1,0:T(1,128)S(1)} %broadcast_in_dim.4), channel_id=1, replica_groups=mesh['sp_0'=16,'sp_1'=4,'dp'=8] {'dp'}, dimensions={0} | all-to-all | bytes 16384 | tf_op jit(solution)/shard_map/all_to_all | solution.py:26
  39.7 0.0 copy-done
  39.7 0.0 copy-done.3
  39.7 2.3 convolution_bitcast_fusion
  42.0 5.1 %copy.21 = f32[4096,192]{1,0:T(8,128)} copy(f32[4096,192]{0,1:T(8,128)} %convolution_bitcast_fusion) | data formatting | bytes 6291456 | tf_op jit(solution)/shard_map/dot_general | solution.py:96
  47.1 4.7 %copy.22 = f32[4,16,64,192]{3,2,1,0:T(8,128)} copy(f32[4,16,64,192]{3,2,0,1:T(8,128)} %bitcast.77) | data formatting | bytes 6291456 | tf_op jit(solution)/shard_map/transpose | solution.py:45
  51.8 0.0 reduce-scatter.3.cloned.1.call-update
  51.8 46.2 %all-gather.8.cloned.1.call-done = bf16[4096,192]{1,0:T(8,128)(2,1)} async-done(((bf16[256,192]{1,0:T(8,128)(2,1)}), bf16[4096,192]{1,0:T(8,128)(2,1)}) %all-gather.8.cloned.1.call-update) | async-done | bytes 1572880 | tf_op jit(solution)/shard_map/all_gather | solution.py:14
  98.0 2.5 %fusion.24 = (f32[192]{0:T(256)S(1)}, f32[128]{0:T(128)S(1)}, f32[128]{0:T(128)S(1)}, f32[128,192]{0,1:T(8,128)S(1)}) fusion(bf16[128,192]{0,1:T(8,128)(2,1)S(1)} %add_convert_fusion, f32[128]{0:T(128)S(1)} %get-tuple-element.81, f32[128]{0:T(128)S(1)} %get-tuple-element.80, f32[192]{0:T(256)S(1)} %copy-done.3, bf16[128,4096]{1,0:T(8,128)(2,1)S(1)} %copy-done, ...), kind=kOutput, calls=%fused_computation.32 | convolution fusion | flops 201768512 | bytes 2772480 | tf_op jit(solution)/shard_map/dot_general | solution.py:75
  100.6 0.6 broadcast_in_dim.5
  101.2 5.1 %all-to-all-start.1 = ((f32[8,1,256]{2,1,0:T(1,128)}), f32[8,1,256]{2,1,0:T(1,128)S(1)}, u32[]{:S(2)}, u32[]{:S(2)}) async-start(f32[8,1,256]{2,1,0:T(1,128)} %broadcast_in_dim.5), calls=%async_computation.1 | async-start | bytes 16384 | tf_op jit(solution)/shard_map/all_to_all | solution.py:26
  106.2 0.0 reduce-scatter.5.cloned.1.call-start
  106.2 1.3 dynamic-slice.1
  107.5 1.3 dynamic-slice
  110.1 0.3 dynamic-update-slice
  110.4 0.0 all-to-all-done.1
  110.4 0.2 reduce-scatter.3.cloned.1.call-done
  110.6 0.0 reduce-scatter.5.cloned.1.call-update
  110.7 0.1 fusion.23
  110.8 1.3 collective-permute-start.1
  112.1 59.2 %all-reduce = f32[3072]{0:T(1024)S(1)} all-reduce(f32[3072]{0:T(1024)S(1)} %dynamic-update-slice), channel_id=4, replica_groups=mesh['sp_0'=16,'sp_1'=4,'dp'=8] {'sp_0'}, use_global_device_ids=true, to_apply=%add | all-reduce | flops 3072 | bytes 24576
  171.3 0.1 reshape.37
  171.4 0.2 dynamic-update-slice.1
  171.6 8.1 %all-reduce.1 = f32[768]{0:T(1024)S(1)} all-reduce(f32[768]{0:T(1024)S(1)} %dynamic-update-slice.1), channel_id=5, replica_groups=mesh['sp_0'=16,'sp_1'=4,'dp'=8] {'sp_1'}, use_global_device_ids=true, to_apply=%add.1 | all-reduce | flops 768 | bytes 6144
  179.7 0.1 reshape.38
  179.7 0.6 reduce_sum.419
  180.3 0.0 collective-permute-done.1
  180.3 1.8 fusion.27
  182.2 0.0 copy-start.1
  182.2 0.0 copy-start.2
  182.2 0.7 multiply_reduce_fusion.18
  182.9 0.7 multiply_reduce_fusion.9
  183.5 0.9 multiply_reduce_fusion
  184.4 0.1 stack.127
  184.5 29.6 %all-gather.4 = f32[16,31,192]{2,1,0:T(8,128)S(1)} all-gather(f32[1,31,192]{2,1,0:T(8,128)S(1)} %bitcast.81), channel_id=2, replica_groups=mesh['sp_0'=16,'sp_1'=4,'dp'=8] {'sp_0'}, dimensions={0}, use_global_device_ids=true | all-gather | bytes 404736 | tf_op jit(solution)/shard_map/all_gather | solution.py:65
  214.2 12.0 %all-gather.5 = f32[4,31,192]{2,1,0:T(8,128)S(1)} all-gather(f32[1,31,192]{2,1,0:T(8,128)S(1)} %bitcast.80), channel_id=3, replica_groups=mesh['sp_0'=16,'sp_1'=4,'dp'=8] {'sp_1'}, dimensions={0}, use_global_device_ids=true | all-gather | bytes 119040 | tf_op jit(solution)/shard_map/all_gather | solution.py:65
  226.2 0.6 reduce_sum.416
  226.8 0.0 copy-done.1
  226.8 0.0 copy-done.2
  226.8 0.7 fusion.5
  227.5 0.0 reduce-scatter.5.cloned.1.call-done
  (13 shorter events, 0.2 us)
Async XLA Ops:
  8.0 31.7 %copy-start = (bf16[128,4096]{1,0:T(8,128)(2,1)S(1)}, bf16[128,4096]{1,0:T(8,128)(2,1)}, u32[]{:S(2)}) copy-start(bf16[128,4096]{1,0:T(8,128)(2,1)} %param.8) | copy-start | bytes 3145732
  8.0 31.7 %copy-start.3 = (f32[192]{0:T(256)S(1)}, f32[192]{0:T(256)}, u32[]{:S(2)}) copy-start(f32[192]{0:T(256)} %param.11) | copy-start | bytes 2308
  8.0 90.0 %all-gather.8.cloned.1.call-start = ((), (), s32[]{:S(2)}) async-start(), calls=%async_computation.4 | async-start | bytes 2228224 | tf_op jit(solution)/shard_map/all_gather | solution.py:14
  22.3 88.3 %reduce-scatter.3.cloned.1.call-start = ((), (), s32[]{:S(2)}) async-start(), calls=%async_computation.5 | async-start | bytes 5242880 | tf_op jit(solution)/shard_map/reduce_scatter | solution.py:48
  23.3 4.6 %collective-permute-start = (bf16[30,192]{0,1:T(8,128)(2,1)S(1)}, bf16[30,192]{0,1:T(8,128)(2,1)S(1)}, u32[]{:S(2)}, u32[]{:S(2)}) collective-permute-start(bf16[30,192]{0,1:T(8,128)(2,1)S(1)} %slice.459), channel_id=1, source_target_pairs={{0,8},{8,16},{16,24},{24,32},{32,40},{40,48},{48,56},{56,64},{64,7... | collective-permute-start | bytes 34568 | tf_op jit(solution)/shard_map/ppermute | solution.py:21
  101.2 9.2 %all-to-all-start.1 = ((f32[8,1,256]{2,1,0:T(1,128)}), f32[8,1,256]{2,1,0:T(1,128)S(1)}, u32[]{:S(2)}, u32[]{:S(2)}) async-start(f32[8,1,256]{2,1,0:T(1,128)} %broadcast_in_dim.5), calls=%async_computation.1 | async-start | bytes 16384 | tf_op jit(solution)/shard_map/all_to_all | solution.py:26
  106.2 121.3 %reduce-scatter.5.cloned.1.call-start = ((), (), s32[]{:S(2)}) async-start(), calls=%async_computation.6 | async-start | bytes 1114112 | tf_op jit(solution)/shard_map/reduce_scatter | solution.py:48
  110.8 69.5 %collective-permute-start.1 = (bf16[30,192]{0,1:T(8,128)(2,1)S(1)}, bf16[30,192]{0,1:T(8,128)(2,1)S(1)}, u32[]{:S(2)}, u32[]{:S(2)}) collective-permute-start(bf16[30,192]{0,1:T(8,128)(2,1)S(1)} %bitcast.79), channel_id=1, source_target_pairs={{8,0},{16,8},{24,16},{32,24},{40,32},{48,40},{56,48},{64,56},{72,6... | collective-permute-start | bytes 34568 | tf_op jit(solution)/shard_map/ppermute | solution.py:21
  182.2 44.7 %copy-start.1 = (bf16[128,192]{0,1:T(8,128)(2,1)S(1)}, bf16[128,192]{0,1:T(8,128)(2,1)}, u32[]{:S(2)}) copy-start(bf16[128,192]{0,1:T(8,128)(2,1)} %param.6) | copy-start | bytes 147460
  182.2 44.7 %copy-start.2 = (bf16[128,192]{0,1:T(8,128)(2,1)S(1)}, bf16[128,192]{0,1:T(8,128)(2,1)}, u32[]{:S(2)}) copy-start(bf16[128,192]{0,1:T(8,128)(2,1)} %param.7) | copy-start | bytes 147460
Sparse Core Ops, SparseCore 0:
  22.4 75.5 all-gather.7
  110.8 71.3 reduce-scatter.4
Sparse Core Ops, SparseCore 1:
  51.9 58.7 reduce-scatter.2
